TPU v7x, 256 devices: a whole 4x4x8 slice. The times are simulated.
256 devices in a mesh: fs: 32 (over z, y), tp: 8 (over x, core).
Axes of the slice: x: 4, y: 4, z: 8, core: 2. Of those that a mesh axis runs over, the one named last changes fastest.
Arguments:
- prompt: bfloat16 [32768, 2048], P(('fs', 'tp')), may hold values from -6 to 6
- norm_gain: float32 [2048], P('fs'), may hold values from 0.1 to 1.9
- up_trained: float32 [2048, 8192], P('fs', 'tp'), may hold values from -0.125 to 0.125
- down_trained: float32 [2048, 8192], P('fs', 'tp'), may hold values from -0.0625 to 0.0625
Outputs:
- up_served: bfloat16 [2048, 8192], P(None, 'tp')
- down_served: bfloat16 [8192, 2048], P('tp')
- mixed: bfloat16 [32768, 2048], P(('fs', 'tp'))
All inputs are finite; a program needn't handle non-finite values.
Results may differ from a plain program's by a relative error of at most 0.014.
Values may be sent and summed in bfloat16 or wider, within the bound.
No kernel may reach another device: no remote copies, remote signals or barrier semaphores. Data moves between devices by JAX's collectives and lax.ppermute only.
A program may use at most 128 MiB of HBM per device.

v0:
```python
import jax
import jax.numpy as jnp
from jax import lax
from jax.sharding import PartitionSpec as P


def sent_together(arrays, axis, dim, along):
    both = jnp.concatenate(arrays, axis=along)
    filled, at, finished = (lax.all_gather(both, axis, axis=dim, tiled=True), 0, [])
    for a in arrays:
        finished.append(lax.slice_in_dim(filled, at, at + a.shape[along], axis=along))
        at += a.shape[along]
    return tuple(finished)


def shards(prompt, norm_gain, up_trained, down_trained):
    up_local = (norm_gain[:, None] * up_trained).astype(jnp.bfloat16)
    down_local = down_trained.astype(jnp.bfloat16)
    values = prompt.astype(jnp.float32)
    scale = lax.rsqrt(jnp.mean(values * values, axis=-1, keepdims=True) + 1e-06)
    normed = (values * scale).astype(jnp.bfloat16)
    group_rows = lax.all_gather(normed, "tp", axis=0, tiled=True)
    up_whole, down_whole = sent_together((up_local, down_local), "fs", 0, 1)
    pre = jnp.dot(group_rows, up_whole, preferred_element_type=jnp.float32)
    hidden = jnp.square(jax.nn.relu(pre)).astype(jnp.bfloat16)
    down_served = jnp.transpose(down_whole)
    mixed = lax.psum_scatter(
        jnp.dot(hidden, down_served, preferred_element_type=jnp.float32).astype(jnp.bfloat16),
        "tp",
        scatter_dimension=0,
        tiled=True,
    )
    return (up_whole, down_served, mixed)


def solution(mesh):
    return jax.shard_map(
        shards,
        mesh=mesh,
        in_specs=(P(("fs", "tp"), None), P("fs"), P("fs", "tp"), P("fs", "tp")),
        out_specs=(P(None, "tp"), P("tp", None), P(("fs", "tp"), None)),
        check_vma=False,
    )
```

profile of v0, /device:TPU:8, one launch (start us, length us, event | category | flops | bytes accessed | tf_op | source)
XLA Modules:
  0.0 207.6 jit_solution(5565873400041753207)
XLA Ops:
  7.2 0.0 all-gather.3.cloned.1.call-start
  7.2 1.0 convert_element_type.19
  8.2 1.0 multiply_convert_fusion.1
  9.2 0.7 pad_maximum_fusion
  9.9 0.0 all-gather.3.cloned.1.call-update
  10.0 0.0 all-gather.5.cloned.1.call-start
  10.0 1.2 fusion.1
  11.3 2.0 fusion.2
  13.2 0.0 all-gather.5.cloned.1.call-update
  13.3 0.0 reduce-scatter.2.cloned.1.call-start
  13.3 97.3 %all-gather.3.cloned.1.call-done = bf16[2048,2048]{1,0:T(8,128)(2,1)} async-done(((bf16[64,2048]{1,0:T(8,128)(2,1)}), bf16[2048,2048]{1,0:T(8,128)(2,1)}) %all-gather.3.cloned.1.call-update) | async-done | bytes 8388624 | tf_op jit(solution)/shard_map/all_gather | solution.py:9
  110.7 6.0 %slice_bitcast_fusion = (bf16[1024,2048]{0,1:T(8,128)(2,1)}, bf16[2048,1024]{1,0:T(8,128)(2,1)}) fusion(bf16[2048,2048]{1,0:T(8,128)(2,1)} %all-gather.3.cloned.1.call-done), kind=kLoop, calls=%fused_computation.3 | loop fusion | bytes 16777216 | tf_op jit(solution)/shard_map/transpose | solution.py:26
  116.7 29.4 %all-gather.5.cloned.1.call-done = bf16[1024,2048]{1,0:T(8,128)(2,1)} async-done(((bf16[128,2048]{1,0:T(8,128)(2,1)}), bf16[1024,2048]{1,0:T(8,128)(2,1)}) %all-gather.5.cloned.1.call-update) | async-done | bytes 4194320 | tf_op jit(solution)/shard_map/all_gather | solution.py:22
  146.0 14.4 %convolution_convert_fusion = bf16[1024,2048]{1,0:T(8,128)(2,1)} fusion(bf16[2048,2048]{1,0:T(8,128)(2,1)} %all-gather.3.cloned.1.call-done, bf16[1024,2048]{1,0:T(8,128)(2,1)} %all-gather.5.cloned.1.call-done, bf16[2048,1024]{1,0:T(8,128)(2,1)} %get-tuple-element.10), kind=kOutput, calls=%fused_computation.1 | convolution fusion | flops 8595177472 | bytes 16777216 | tf_op jit(solution)/shard_map/dot_general | solution.py:28
  160.4 0.0 reduce-scatter.2.cloned.1.call-update
  160.4 6.4 %copy.10 = bf16[1024,2048]{1,0:T(8,128)(2,1)} copy(bf16[1024,2048]{0,1:T(8,128)(2,1)} %get-tuple-element.9) | data formatting | bytes 8388608
  166.9 34.2 %reduce-scatter.2.cloned.1.call-done = bf16[128,2048]{1,0:T(8,128)(2,1)} async-done(((bf16[1024,2048]{1,0:T(8,128)(2,1)}), bf16[128,2048]{1,0:T(8,128)(2,1)}) %reduce-scatter.2.cloned.1.call-update) | async-done | bytes 524304 | tf_op jit(solution)/shard_map/reduce_scatter | solution.py:27
  (1 shorter events, 0.0 us)
Async XLA Ops:
  7.2 103.5 %all-gather.3.cloned.1.call-start = ((), (), s32[]{:S(2)}) async-start(), calls=%async_computation.1 | async-start | bytes 8650752 | tf_op jit(solution)/shard_map/all_gather | solution.py:9
  10.0 136.1 %all-gather.5.cloned.1.call-start = ((), (), s32[]{:S(2)}) async-start(), calls=%async_computation.2 | async-start | bytes 4718592 | tf_op jit(solution)/shard_map/all_gather | solution.py:22
  13.3 187.8 %reduce-scatter.2.cloned.1.call-start = ((), (), s32[]{:S(2)}) async-start(), calls=%async_computation.3 | async-start | bytes 4718592 | tf_op jit(solution)/shard_map/reduce_scatter | solution.py:27
Sparse Core Ops, SparseCore 0:
  11.1 99.4 all-gather.2
  113.1 32.8 all-gather.4
  160.5 40.4 reduce-scatter.1
where the time goes:
time: 208 us
  waiting for transfers between devices  161 us (77%)
  matrix products  14.4 us (7%)
  between operations  13.8 us (7%)
  local copies, waits for them, and re-layouts  12.5 us (6%)
  other arithmetic  5.96 us (3%)
    all_gather x1, waiting for transfers between devices, sent_together(): lax.all_gather(both, axis, axis=dim, tiled=True)  97.3 us
    reduce_scatter x1, waiting for transfers between devices, shards(): lax.psum_scatter(jnp.dot(hidden, down_served, preferred_element_type=jnp....  34.2 us
    all_gather x1, waiting for transfers between devices, shards(): group_rows = lax.all_gather(normed, 'tp', axis=0, tiled=True)  29.4 us
    dot_general x1, matrix products, shards(): jnp.dot(hidden, down_served, preferred_element_type=jnp.float32)  14.4 us
    unnamed x1, local copies, waits for them, and re-layouts  6.43 us
    transpose x1, local copies, waits for them, and re-layouts, shards(): down_served = jnp.transpose(down_whole)  6.02 us
  transfers between devices with their start and end apart: 3, of which 3 were waited for; matrix products, arithmetic and copies ran while one was open for 8% of the time, Pallas kernels for 0%

commit v1 on v0

--- a/solution.py
+++ b/solution.py
@@ -19,7 +19,8 @@
     values = prompt.astype(jnp.float32)
     scale = lax.rsqrt(jnp.mean(values * values, axis=-1, keepdims=True) + 1e-06)
     normed = (values * scale).astype(jnp.bfloat16)
-    group_rows = lax.all_gather(normed, "tp", axis=0, tiled=True)
+    copies = jnp.concatenate([normed] * lax.axis_size("tp"), axis=0)
+    group_rows = lax.all_to_all(copies, "tp", 0, 0, tiled=True)
     up_whole, down_whole = sent_together((up_local, down_local), "fs", 0, 1)
     pre = jnp.dot(group_rows, up_whole, preferred_element_type=jnp.float32)
     hidden = jnp.square(jax.nn.relu(pre)).astype(jnp.bfloat16)

time: 208 us -> 177 us (0.85)
  waiting for transfers between devices: 161 us -> 122 us
  starting transfers between devices: 0.12 us -> 4.67 us
    all_gather x1 -> x0, waiting for transfers between devices: 29.4 us -> none  [shards(): group_rows = lax.all_gather(normed, 'tp', axis=0, tiled=True)]
    all_gather x1, waiting for transfers between devices: 97.3 us -> 89.5 us  [sent_together(): lax.all_gather(both, axis, axis=dim, tiled=True)]
    all_to_all x0 -> x1, starting transfers between devices: none -> 4.59 us  [shards(): group_rows = lax.all_to_all(copies, 'tp', 0, 0, tiled=True)]
    unnamed x0 -> x7, other arithmetic: none -> 3.18 us
    unnamed x1 -> x5, local copies, waits for them, and re-layouts: 6.43 us -> 8.45 us
  transfers between devices with their start and end apart: 3 -> 3, of which waited for: 3 -> 2; matrix products, arithmetic and copies ran while one was open for 8% -> 10% of each run, Pallas kernels for 0% -> 0%
where the time goes in v1:
time: 177 us
  waiting for transfers between devices  122 us (69%)
  local copies, waits for them, and re-layouts  14.5 us (8%)
  matrix products  14.4 us (8%)
  between operations  14.1 us (8%)
  other arithmetic  7.35 us (4%)
  starting transfers between devices  4.67 us (3%)
    all_gather x1, waiting for transfers between devices, sent_together(): lax.all_gather(both, axis, axis=dim, tiled=True)  89.5 us
    reduce_scatter x1, waiting for transfers between devices, shards(): lax.psum_scatter(jnp.dot(hidden, down_served, preferred_element_type=jnp....  32.5 us
    dot_general x1, matrix products, shards(): jnp.dot(hidden, down_served, preferred_element_type=jnp.float32)  14.4 us
    unnamed x5, local copies, waits for them, and re-layouts  8.45 us
    transpose x1, local copies, waits for them, and re-layouts, shards(): down_served = jnp.transpose(down_whole)  6.02 us
    all_to_all x1, starting transfers between devices, shards(): group_rows = lax.all_to_all(copies, 'tp', 0, 0, tiled=True)  4.59 us
  transfers between devices with their start and end apart: 3, of which 2 were waited for; matrix products, arithmetic and copies ran while one was open for 10% of the time, Pallas kernels for 0%

profile of v1, /device:TPU:8, one launch (start us, length us, event | category | flops | bytes accessed | tf_op | source)
XLA Modules:
  0.0 176.9 jit_solution(13976503917289991912)
XLA Ops:
  7.2 0.0 all-gather.2.cloned.1.call-start
  7.2 1.0 convert_element_type.19
  8.2 1.0 multiply_convert_fusion.1
  9.3 0.7 pad_maximum_fusion
  10.0 0.0 all-gather.2.cloned.1.call-update
  10.0 1.2 fusion.1
  11.3 1.2 constant_dynamic-update-slice_fusion.7
  12.5 1.2 constant_dynamic-update-slice_fusion.6
  13.7 0.2 constant_dynamic-update-slice_fusion.5
  13.8 0.2 constant_dynamic-update-slice_fusion.4
  14.0 0.2 constant_dynamic-update-slice_fusion.3
  14.2 0.2 constant_dynamic-update-slice_fusion.2
  14.3 0.2 constant_dynamic-update-slice_fusion.1
  14.5 0.2 constant_dynamic-update-slice_fusion
  14.6 0.0 copy-start.1
  14.6 2.0 %copy-done.1 = bf16[1024,2048]{1,0:T(8,128)(2,1)} copy-done((bf16[1024,2048]{1,0:T(8,128)(2,1)}, bf16[1024,2048]{1,0:T(8,128)(2,1)S(1)}, u32[]{:S(2)}) %copy-start.1) | copy-done | bytes 4194328
  16.7 4.6 %all-to-all-start = ((bf16[8,128,2048]{2,1,0:T(8,128)(2,1)}), bf16[8,128,2048]{2,1,0:T(8,128)(2,1)}, u32[]{:S(2)}, u32[]{:S(2)}) async-start(bf16[8,128,2048]{2,1,0:T(8,128)(2,1)} %bitcast.6), calls=%async_computation | async-start | bytes 8388608 | tf_op jit(solution)/shard_map/all_to_all | solution.py:23
  21.3 0.0 reduce-scatter.2.cloned.1.call-start
  21.3 89.5 %all-gather.2.cloned.1.call-done = bf16[2048,2048]{1,0:T(8,128)(2,1)} async-done(((bf16[64,2048]{1,0:T(8,128)(2,1)}), bf16[2048,2048]{1,0:T(8,128)(2,1)}) %all-gather.2.cloned.1.call-update) | async-done | bytes 8388624 | tf_op jit(solution)/shard_map/all_gather | solution.py:9
  110.8 6.0 %slice_bitcast_fusion = (bf16[1024,2048]{0,1:T(8,128)(2,1)}, bf16[2048,1024]{1,0:T(8,128)(2,1)}) fusion(bf16[2048,2048]{1,0:T(8,128)(2,1)} %all-gather.2.cloned.1.call-done), kind=kLoop, calls=%fused_computation.3 | loop fusion | bytes 16777216 | tf_op jit(solution)/shard_map/transpose | solution.py:27
  116.8 14.4 %convolution_convert_fusion = bf16[1024,2048]{1,0:T(8,128)(2,1)} fusion(bf16[2048,2048]{1,0:T(8,128)(2,1)} %all-gather.2.cloned.1.call-done, bf16[1024,2048]{1,0:T(8,128)(2,1)} %bitcast.2, bf16[2048,1024]{1,0:T(8,128)(2,1)} %get-tuple-element.10), kind=kOutput, calls=%fused_computation.1 | convolution fusion | flops 8595177472 | bytes 16777216 | tf_op jit(solution)/shard_map/dot_general | solution.py:29
  131.2 0.0 reduce-scatter.2.cloned.1.call-update
  131.2 6.4 %copy.10 = bf16[1024,2048]{1,0:T(8,128)(2,1)} copy(bf16[1024,2048]{0,1:T(8,128)(2,1)} %get-tuple-element.9) | data formatting | bytes 8388608
  137.6 32.5 %reduce-scatter.2.cloned.1.call-done = bf16[128,2048]{1,0:T(8,128)(2,1)} async-done(((bf16[1024,2048]{1,0:T(8,128)(2,1)}), bf16[128,2048]{1,0:T(8,128)(2,1)}) %reduce-scatter.2.cloned.1.call-update) | async-done | bytes 524304 | tf_op jit(solution)/shard_map/reduce_scatter | solution.py:28
  (4 shorter events, 0.0 us)
Async XLA Ops:
  7.2 6.5 %copy-start = (bf16[128,2048]{1,0:T(8,128)(2,1)S(1)}, bf16[128,2048]{1,0:T(8,128)(2,1)}, u32[]{:S(2)}) copy-start(bf16[128,2048]{1,0:T(8,128)(2,1)} %param.4) | copy-start | bytes 1572868
  7.2 103.6 %all-gather.2.cloned.1.call-start = ((), (), s32[]{:S(2)}) async-start(), calls=%async_computation.2 | async-start | bytes 8650752 | tf_op jit(solution)/shard_map/all_gather | solution.py:9
  14.6 2.0 %copy-start.1 = (bf16[1024,2048]{1,0:T(8,128)(2,1)}, bf16[1024,2048]{1,0:T(8,128)(2,1)S(1)}, u32[]{:S(2)}) copy-start(bf16[1024,2048]{1,0:T(8,128)(2,1)S(1)} %constant_dynamic-update-slice_fusion) | copy-start | bytes 12582916
  16.7 100.2 %all-to-all-start = ((bf16[8,128,2048]{2,1,0:T(8,128)(2,1)}), bf16[8,128,2048]{2,1,0:T(8,128)(2,1)}, u32[]{:S(2)}, u32[]{:S(2)}) async-start(bf16[8,128,2048]{2,1,0:T(8,128)(2,1)} %bitcast.6), calls=%async_computation | async-start | bytes 8388608 | tf_op jit(solution)/shard_map/all_to_all | solution.py:23
  21.3 148.8 %reduce-scatter.2.cloned.1.call-start = ((), (), s32[]{:S(2)}) async-start(), calls=%async_computation.3 | async-start | bytes 4718592 | tf_op jit(solution)/shard_map/reduce_scatter | solution.py:28
Sparse Core Ops, SparseCore 0:
  11.1 99.6 all-gather.1
  131.3 38.7 reduce-scatter.1
